TPU v7x, 32 devices: a whole 2x2x4 slice. The times are simulated.
32 devices in a mesh: ep: 8 (over z, x), tp: 4 (over y, core).
Axes of the slice: x: 2, y: 2, z: 4, core: 2. Of those that a mesh axis runs over, the one named last changes fastest.
Arguments:
- conv_value: bfloat16 [4096, 2048], P('ep', 'tp'), may hold values from -6 to 6
- conv_gate: bfloat16 [4096, 2048], P('ep', 'tp'), may hold values from -9 to 9
- conv_taps: float32 [31, 2048], P(None, 'tp'), may hold values from -14 to 14
- norm_gain: float32 [2048], P('tp'), may hold values from 0.1 to 1.9
- norm_shift: float32 [2048], P('tp'), may hold values from -3 to 3
- conv_out_weight: bfloat16 [2048, 2048], P(None, 'tp'), may hold values from -0.125 to 0.125
- moe_input: bfloat16 [1024, 2048], P('ep'), may hold values from -6 to 6
- moe_gain: float32 [2048], replicated, may hold values from 0.1 to 1.9
- routes: int32 [1024, 4], P('ep'), may hold values from 0 to 7, all different within a row; in each aligned block of 128 rows (0 to 127, 128 to 255, ...) at most 128 rows name the same one
- route_weights: float32 [1024, 4], P('ep'), may hold values from 0.25 to 1
- expert_gate: bfloat16 [8, 2048, 4096], P('ep', None, 'tp'), may hold values from -0.125 to 0.125
- expert_up: bfloat16 [8, 2048, 4096], P('ep', None, 'tp'), may hold values from -0.125 to 0.125
- expert_down: bfloat16 [8, 4096, 2048], P('ep', None, 'tp'), may hold values from -0.09375 to 0.09375
- shared_gate: bfloat16 [2048, 512], P(None, 'tp'), may hold values from -0.125 to 0.125
- shared_up: bfloat16 [2048, 512], P(None, 'tp'), may hold values from -0.125 to 0.125
- shared_down: bfloat16 [512, 2048], P(None, 'tp'), may hold values from -0.25 to 0.25
Outputs:
- conv_result: bfloat16 [4096, 2048], P('ep', 'tp')
- moe_result: bfloat16 [1024, 2048], P('ep', 'tp')
Inputs may be any that keep to these rules, and one draw needn't show every extreme that they name: `routes`: in the rows of one device (aligned blocks of 128 rows) no expert is named by more than 128 rows, a bound that some block reaches; each row names 4 different experts.
All inputs are finite; a program needn't handle non-finite values.
Results may differ from a plain program's by a relative error of at most 0.0068.
Values may be sent and summed in bfloat16 or wider, within the bound.
A program may use at most 64 MiB of HBM per device.

v0:
```python
import jax
import jax.numpy as jnp
from jax import lax
from jax.sharding import PartitionSpec as P


def from_behind(value, axis, steps):
    count = lax.axis_size(axis)
    initial, last = (max(0, -steps), min(count, count - steps))
    return lax.ppermute(value, axis, [(source, source + steps) for source in range(initial, last)])


def body(
    conv_value,
    conv_gate,
    conv_taps,
    norm_gain,
    norm_shift,
    conv_out_weight,
    moe_input,
    moe_gain,
    routes,
    route_weights,
    expert_gate,
    expert_up,
    expert_down,
    shared_gate,
    shared_up,
    shared_down,
):
    tap_count = conv_taps.shape[0]
    rows_a = conv_value.shape[0]
    glu_rows = (
        conv_value.astype(jnp.float32) * jax.nn.sigmoid(conv_gate.astype(jnp.float32))
    ).astype(jnp.bfloat16)
    before = from_behind(glu_rows[rows_a - (tap_count - 1) :], "ep", 1)
    padded = jnp.concatenate([before, glu_rows], axis=0)
    filtered = jnp.zeros(glu_rows.shape, jnp.float32)
    for offset in range(tap_count):
        filtered = filtered + conv_taps[offset] * padded[offset : offset + rows_a].astype(
            jnp.float32
        )
    row_total, squares = lax.psum(
        (jnp.sum(filtered, axis=1), jnp.sum(filtered * filtered, axis=1)), "tp"
    )
    channels = conv_out_weight.shape[0]
    row_mean = row_total / channels
    row_square = squares / channels
    scaled = (filtered - row_mean[:, None]) * lax.rsqrt(row_square - row_mean * row_mean + 1e-05)[
        :, None
    ]
    conv_hidden = jax.nn.silu(scaled * norm_gain + norm_shift).astype(jnp.bfloat16)
    conv_sum = jnp.dot(
        lax.all_gather(conv_hidden, "tp", axis=1, tiled=True),
        conv_out_weight,
        preferred_element_type=jnp.float32,
    )
    conv_result = conv_sum.astype(jnp.bfloat16)
    inputs = moe_input.astype(jnp.float32)
    normed = (
        inputs * lax.rsqrt(jnp.mean(inputs * inputs, axis=1, keepdims=True) + 1e-06) * moe_gain
    ).astype(jnp.bfloat16)
    rows_b, per_row = routes.shape
    model_width = normed.shape[1]
    groups = lax.axis_size("ep")
    capacity = 2 * rows_b * per_row // groups
    flat_expert = routes.reshape(-1)
    owner_row = jnp.arange(rows_b * per_row, dtype=jnp.int32) // per_row
    expert_hits = (flat_expert[:, None] == jnp.arange(groups, dtype=jnp.int32)[None, :]).astype(
        jnp.int32
    )
    slot_rank = jnp.sum((jnp.cumsum(expert_hits, axis=0) - expert_hits) * expert_hits, axis=1)
    slot_index = flat_expert * capacity + slot_rank
    outgoing = (
        jnp.zeros((groups * capacity, model_width), jnp.bfloat16)
        .at[slot_index]
        .set(normed[owner_row])
    )
    outgoing = outgoing.reshape(groups, capacity, model_width)
    slot_share = capacity // lax.axis_size("tp")
    own_slots = lax.dynamic_slice_in_dim(outgoing, lax.axis_index("tp") * slot_share, slot_share, 1)
    partial_rows = lax.all_to_all(own_slots, "ep", split_axis=0, concat_axis=0, tiled=True)
    arrived = lax.all_gather(partial_rows, "tp", axis=1, tiled=True)
    arrived_rows = arrived.reshape(groups * capacity, model_width)
    gate_value = jnp.dot(arrived_rows, expert_gate[0], preferred_element_type=jnp.float32)
    upward = jnp.dot(arrived_rows, expert_up[0], preferred_element_type=jnp.float32)
    expert_hidden = (jax.nn.silu(gate_value) * upward).astype(jnp.bfloat16)
    shared_hidden = (
        jax.nn.silu(jnp.dot(normed, shared_gate, preferred_element_type=jnp.float32))
        * jnp.dot(normed, shared_up, preferred_element_type=jnp.float32)
    ).astype(jnp.bfloat16)
    columns = expert_down.shape[2]
    routed_rows = expert_down[0]
    routed_sum = jnp.dot(
        lax.all_gather(expert_hidden, "tp", axis=1, tiled=True),
        routed_rows,
        preferred_element_type=jnp.float32,
    )
    shared_sum = jnp.dot(
        lax.all_gather(shared_hidden, "tp", axis=1, tiled=True),
        shared_down,
        preferred_element_type=jnp.float32,
    )
    expert_out = routed_sum.astype(jnp.bfloat16).reshape(groups, capacity, columns)
    returned = lax.all_to_all(expert_out, "ep", split_axis=0, concat_axis=0, tiled=True).reshape(
        groups * capacity, columns
    )
    picked = returned[slot_index].astype(jnp.float32) * route_weights.reshape(-1)[:, None]
    moe_sum = jnp.sum(picked.reshape(rows_b, per_row, columns), axis=1) + shared_sum
    return (conv_result, moe_sum.astype(jnp.bfloat16))


def solution(mesh):
    return jax.shard_map(
        body,
        mesh=mesh,
        in_specs=(
            P("ep", "tp"),
            P("ep", "tp"),
            P(None, "tp"),
            P("tp"),
            P("tp"),
            P(None, "tp"),
            P("ep", None),
            P(),
            P("ep", None),
            P("ep", None),
            P("ep", None, "tp"),
            P("ep", None, "tp"),
            P("ep", None, "tp"),
            P(None, "tp"),
            P(None, "tp"),
            P(None, "tp"),
        ),
        out_specs=(P("ep", "tp"), P("ep", "tp")),
        check_vma=False,
    )
```

profile of v0, /device:TPU:0, one launch (start us, length us, event | category | flops | bytes accessed | tf_op | source)
XLA Modules:
  0.0 221.6 jit_solution(14922758619860375159)
XLA Ops:
  7.2 0.8 broadcast_multiply_fusion
  8.1 0.8 copy.20
  9.1 1.2 fusion.16
  10.6 1.1 reduce-window.6
  11.7 0.2 slice_reduce_fusion
  12.1 1.2 fusion.18
  13.3 12.8 %scatter_custom_fusion = bf16[1024,2048]{1,0:T(8,128)(2,1)} fusion(s32[512]{0:T(512)S(1)} %bitcast.105, bf16[128,2048]{1,0:T(8,128)(2,1)S(1)} %fusion.18, s32[1024]{0:T(1024)S(1)} %pad_clamp_fusion.1, bf16[]{:T(256)} %constant.46.clone.1), kind=kCustom, calls=%fused_computation.39 | custom fusion | bytes 4194306 | tf_op jit(solution)/shard_map/scatter | solution.py:77
  26.1 1.3 constant_dynamic-slice_fusion
  27.4 32.9 %all_to_all.10 = bf16[8,32,2048]{2,1,0:T(8,128)(2,1)} all-to-all(bf16[8,32,2048]{2,1,0:T(8,128)(2,1)S(1)} %constant_dynamic-slice_fusion), channel_id=1, replica_groups=mesh['ep'=8,'tp'=4] {'ep'}, dimensions={0} | all-to-all | bytes 2097152 | tf_op jit(solution)/shard_map/all_to_all | solution.py:82
  60.4 33.6 %all-gather.6.cloned.1.call-done = bf16[8,128,2048]{2,1,0:T(8,128)(2,1)} async-done(((bf16[8,32,2048]{2,1,0:T(8,128)(2,1)}), bf16[8,128,2048]{2,1,0:T(8,128)(2,1)}) %all-gather.6.cloned.1.call-update) | async-done | bytes 4194320 | tf_op jit(solution)/shard_map/all_gather | solution.py:83
  94.0 7.6 %fusion.2 = f32[1024,1024]{1,0:T(8,128)S(1)} fusion(bf16[1024,2048]{1,0:T(8,128)(2,1)} %bitcast.109, bf16[1,2048,1024]{2,1,0:T(8,128)(2,1)} %param.27), kind=kOutput, calls=%fused_computation.34 | convolution fusion | flops 4294967296 | bytes 12582912 | tf_op jit(solution)/shard_map/dot_general | solution.py:86
  101.8 6.3 %multiply_convert_fusion = bf16[1024,1024]{1,0:T(8,128)(2,1)} fusion(f32[1024,1024]{1,0:T(8,128)S(1)} %fusion.2, bf16[1024,2048]{1,0:T(8,128)(2,1)S(1)} %bitcast.110, bf16[1,2048,1024]{2,1,0:T(8,128)(2,1)S(1)} %copy-done.8), kind=kOutput, calls=%fused_computation.38 | convolution fusion | flops 4301258752 | bytes 14680064 | tf_op jit(solution)/shard_map/dot_general | solution.py:85
  108.2 0.3 multiply_convert_fusion.2
  108.5 3.4 %collective-permute-start = (bf16[30,512]{1,0:T(8,128)(2,1)S(1)}, bf16[30,512]{1,0:T(8,128)(2,1)S(1)}, u32[]{:S(2)}, u32[]{:S(2)}) collective-permute-start(bf16[30,512]{1,0:T(8,128)(2,1)S(1)} %slice.260), channel_id=1, source_target_pairs={{0,4},{4,8},{8,12},{12,16},{16,20},{20,24},{24,28},{1,5},{5,9},{9,... | collective-permute-start | bytes 92168 | tf_op jit(solution)/shard_map/ppermute | solution.py:10
  112.0 1.5 collective-permute-done
  113.5 4.8 %fusion.51 = (f32[512]{0:T(512)S(1)}, f32[512]{0:T(512)S(1)}, f32[512,512]{1,0:T(8,128)S(1)}) fusion(bf16[512,512]{1,0:T(8,128)(2,1)S(1)} %multiply_convert_fusion.2, f32[512]{0:T(512)S(1)} %bitcast.103, bf16[30,512]{1,0:T(8,128)(2,1)S(1)} %collective-permute-done, f32[512]{0:T(512)S(1)} %bitcast.104, f32[512]{0:T(512)S(1)} %bitcast.75, ...), kind=kLoop, calls=%fused_computation.113 | loop fusion | flops 48495616 | bytes 1671168 | tf_op jit(solution)/shard_map/reduce_sum | solution.py:44
  118.3 6.5 %all-reduce = (f32[512]{0:T(512)S(1)}, f32[512]{0:T(512)S(1)}) all-reduce(f32[512]{0:T(512)S(1)} %get-tuple-element.3, f32[512]{0:T(512)S(1)} %get-tuple-element.2), channel_id=1, replica_groups=mesh['ep'=8,'tp'=4] {'tp'}, use_global_device_ids=true, to_apply=%region_3.0 | all-reduce | flops 1024 | bytes 8192 | tf_op jit(solution)/shard_map/psum | solution.py:43
  124.8 1.2 multiply_convert_fusion.1
  126.1 40.6 %all-gather.8.cloned.1.call-done = bf16[1024,4096]{1,0:T(8,128)(2,1)} async-done(((bf16[1024,1024]{1,0:T(8,128)(2,1)}), bf16[1024,4096]{1,0:T(8,128)(2,1)}) %all-gather.8.cloned.1.call-update) | async-done | bytes 8388624 | tf_op jit(solution)/shard_map/all_gather | solution.py:95
  166.7 10.0 %fusion.11 = bf16[1024,512]{1,0:T(8,128)(2,1)} fusion(bf16[1024,4096]{1,0:T(8,128)(2,1)} %all-gather.8.cloned.1.call-done, bf16[1,4096,512]{2,1,0:T(8,128)(2,1)} %param.28), kind=kOutput, calls=%fused_computation.42 | convolution fusion | flops 4295491584 | bytes 13631488 | tf_op jit(solution)/shard_map/dot_general | solution.py:94
  176.7 5.5 %all-to-all-start.1 = ((bf16[8,128,512]{2,1,0:T(8,128)(2,1)}), bf16[8,128,512]{2,1,0:T(8,128)(2,1)S(1)}, u32[]{:S(2)}, u32[]{:S(2)}) async-start(bf16[8,128,512]{2,1,0:T(8,128)(2,1)} %bitcast.73), calls=%async_computation.1 | async-start | bytes 2097152 | tf_op jit(solution)/shard_map/all_to_all | solution.py:105
  182.2 0.1 copy.22
  182.3 1.5 fusion.54
  183.8 1.5 fusion.15
  185.3 6.1 %all_gather.15 = bf16[128,512]{1,0:T(8,128)(2,1)S(1)} all-gather(bf16[128,128]{1,0:T(8,128)(2,1)S(1)} %fusion.15), channel_id=1, replica_groups=mesh['ep'=8,'tp'=4] {'tp'}, dimensions={1}, use_global_device_ids=true | all-gather | bytes 163840 | tf_op jit(solution)/shard_map/all_gather | solution.py:100
  191.4 0.7 all-gather.4.cloned.1.call-done
  192.1 3.6 %convolution_convert_fusion = bf16[512,512]{1,0:T(8,128)(2,1)} fusion(bf16[512,2048]{1,0:T(8,128)(2,1)} %all-gather.4.cloned.1.call-done, bf16[2048,512]{1,0:T(8,128)(2,1)S(1)} %copy-done), kind=kOutput, calls=%fused_computation.45 | convolution fusion | flops 1074003968 | bytes 4718592 | tf_op jit(solution)/shard_map/dot_general | solution.py:53
  195.7 12.7 %all-to-all-done.1 = bf16[8,128,512]{2,1,0:T(8,128)(2,1)S(1)} async-done(((bf16[8,128,512]{2,1,0:T(8,128)(2,1)}), bf16[8,128,512]{2,1,0:T(8,128)(2,1)S(1)}, u32[]{:S(2)}, u32[]{:S(2)}) %all-to-all-start.1) | async-done | bytes 1048608 | tf_op jit(solution)/shard_map/all_to_all | solution.py:105
  208.4 2.6 %gather_fusion = bf16[512,512]{1,0:T(8,128)(2,1)} fusion(bf16[1024,512]{1,0:T(8,128)(2,1)S(1)} %bitcast.71, s32[1024]{0:T(1024)S(1)} %pad_clamp_fusion), kind=kCustom, calls=%fused_computation.1 | custom fusion | bytes 1050624 | tf_op jit(solution)/shard_map/gather | solution.py:108
  211.0 1.4 reshape.133
  212.4 0.7 multiply_reduce_fusion
  213.1 1.9 fusion.14
  (43 shorter events, 0.9 us)
Async XLA Ops:
  7.2 184.9 %copy-start = (bf16[2048,512]{1,0:T(8,128)(2,1)S(1)}, bf16[2048,512]{1,0:T(8,128)(2,1)}, u32[]{:S(2)}) copy-start(bf16[2048,512]{1,0:T(8,128)(2,1)} %param.21) | copy-start | bytes 6291460
  7.2 86.9 %all-gather.6.cloned.1.call-start = ((), (), s32[]{:S(2)}) async-start(), calls=%async_computation.3 | async-start | bytes 5242880 | tf_op jit(solution)/shard_map/all_gather | solution.py:83
  13.3 47.1 %copy-start.1 = (bf16[128,2048]{1,0:T(8,128)(2,1)}, bf16[128,2048]{1,0:T(8,128)(2,1)S(1)}, u32[]{:S(2)}) copy-start(bf16[128,2048]{1,0:T(8,128)(2,1)S(1)} %fusion.18) | copy-start | bytes 1572868
  60.4 106.3 %all-gather.8.cloned.1.call-start = ((), (), s32[]{:S(2)}) async-start(), calls=%async_computation.4 | async-start | bytes 10485760 | tf_op jit(solution)/shard_map/all_gather | solution.py:95
  94.0 7.7 %copy-start.8 = (bf16[1,2048,1024]{2,1,0:T(8,128)(2,1)S(1)}, bf16[1,2048,1024]{2,1,0:T(8,128)(2,1)}, u32[]{:S(2)}) copy-start(bf16[1,2048,1024]{2,1,0:T(8,128)(2,1)} %param.26) | copy-start | bytes 12582916
  94.0 7.7 %copy-start.9 = (bf16[8,128,2048]{2,1,0:T(8,128)(2,1)S(1)}, bf16[8,128,2048]{2,1,0:T(8,128)(2,1)}, u32[]{:S(2)}) copy-start(bf16[8,128,2048]{2,1,0:T(8,128)(2,1)} %all-gather.6.cloned.1.call-done) | copy-start | bytes 12582916
  101.7 6.4 %copy-start.2 = (bf16[512,512]{1,0:T(8,128)(2,1)S(1)}, bf16[512,512]{1,0:T(8,128)(2,1)}, u32[]{:S(2)}) copy-start(bf16[512,512]{1,0:T(8,128)(2,1)} %param.17) | copy-start | bytes 1572868
  101.7 6.4 %copy-start.3 = (bf16[512,512]{1,0:T(8,128)(2,1)S(1)}, bf16[512,512]{1,0:T(8,128)(2,1)}, u32[]{:S(2)}) copy-start(bf16[512,512]{1,0:T(8,128)(2,1)} %param.16) | copy-start | bytes 1572868
  101.7 10.1 %copy-start.4 = (f32[31,512]{1,0:T(8,128)S(1)}, f32[31,512]{1,0:T(8,128)}, u32[]{:S(2)}) copy-start(f32[31,512]{1,0:T(8,128)} %param.18) | copy-start | bytes 190468
  108.1 16.7 %copy-start.5 = (f32[512]{0:T(512)S(1)}, f32[512]{0:T(512)}, u32[]{:S(2)}) copy-start(f32[512]{0:T(512)} %param.20) | copy-start | bytes 6148
  108.1 16.7 %copy-start.6 = (f32[512]{0:T(512)S(1)}, f32[512]{0:T(512)}, u32[]{:S(2)}) copy-start(f32[512]{0:T(512)} %param.19) | copy-start | bytes 6148
  108.1 84.0 %all-gather.4.cloned.1.call-start = ((), (), s32[]{:S(2)}) async-start(), calls=%async_computation.2 | async-start | bytes 2621440 | tf_op jit(solution)/shard_map/all_gather | solution.py:54
  108.5 5.0 %collective-permute-start = (bf16[30,512]{1,0:T(8,128)(2,1)S(1)}, bf16[30,512]{1,0:T(8,128)(2,1)S(1)}, u32[]{:S(2)}, u32[]{:S(2)}) collective-permute-start(bf16[30,512]{1,0:T(8,128)(2,1)S(1)} %slice.260), channel_id=1, source_target_pairs={{0,4},{4,8},{8,12},{12,16},{16,20},{20,24},{24,28},{1,5},{5,9},{9,... | collective-permute-start | bytes 92168 | tf_op jit(solution)/shard_map/ppermute | solution.py:10
  126.1 56.1 %copy-start.7 = (f32[128,4]{0,1:T(4,128)S(1)}, f32[128,4]{0,1:T(4,128)}, u32[]{:S(2)}) copy-start(f32[128,4]{0,1:T(4,128)} %param.25) | copy-start | bytes 6148
  176.7 31.7 %all-to-all-start.1 = ((bf16[8,128,512]{2,1,0:T(8,128)(2,1)}), bf16[8,128,512]{2,1,0:T(8,128)(2,1)S(1)}, u32[]{:S(2)}, u32[]{:S(2)}) async-start(bf16[8,128,512]{2,1,0:T(8,128)(2,1)} %bitcast.73), calls=%async_computation.1 | async-start | bytes 2097152 | tf_op jit(solution)/shard_map/all_to_all | solution.py:105
Sparse Core Ops, SparseCore 0:
  60.5 33.4 all-gather.5
  108.2 58.3 all-gather.7
  168.8 23.2 all-gather.3
where the time goes:
time: 222 us
  waiting for transfers between devices  89.1 us (40%)
  blocking collectives  45.5 us (20%)
  matrix products  32.5 us (15%)
  local copies, waits for them, and re-layouts  19.8 us (9%)
  between operations  14 us (6%)
  other arithmetic  11.7 us (5%)
  starting transfers between devices  9.02 us (4%)
    all_gather x1, waiting for transfers between devices, body(): lax.all_gather(expert_hidden, 'tp', axis=1, tiled=True)  40.6 us
    all_gather x1, waiting for transfers between devices, body(): arrived = lax.all_gather(partial_rows, 'tp', axis=1, tiled=True)  33.6 us
    all_to_all x1, blocking collectives, body(): lax.all_to_all(own_slots, 'ep', split_axis=0, concat_axis=0, tiled=True)  32.9 us
    scatter x1, local copies, waits for them, and re-layouts, body(): outgoing = jnp.zeros((groups * capacity, model_width), jnp.bfloat16).at[s...  12.8 us
    all_to_all x1, waiting for transfers between devices, body(): lax.all_to_all(expert_out, 'ep', split_axis=0, concat_axis=0, tiled=True)  12.7 us
    dot_general x1, matrix products, body(): jnp.dot(lax.all_gather(expert_hidden, 'tp', axis=1, tiled=True), routed_r...  10 us
    dot_general x1, matrix products, body(): jnp.dot(arrived_rows, expert_up[0], preferred_element_type=jnp.float32)  7.64 us
    psum x1, blocking collectives, body(): lax.psum((jnp.sum(filtered, axis=1), jnp.sum(filtered * filtered, axis=1)...  6.48 us
  transfers between devices with their start and end apart: 5, of which 5 were waited for; matrix products, arithmetic and copies ran while one was open for 10% of the time, Pallas kernels for 0%

commit v1 on v0

v1 whole, which is shorter than its diff:
```python
import functools

import jax
import jax.numpy as jnp
from jax import lax
from jax.experimental import pallas as pl
from jax.experimental.pallas import tpu as pltpu
from jax.sharding import PartitionSpec as P

MESH = pl.DeviceIdType.MESH
TILES = 2


def from_behind(value, axis, steps):
    count = lax.axis_size(axis)
    initial, last = (max(0, -steps), min(count, count - steps))
    return lax.ppermute(value, axis, [(source, source + steps) for source in range(initial, last)])


def silu(v):
    return v / (1.0 + jnp.exp(-v))


def moe_kernel(
    depth,
    normed,
    weights,
    gate_hbm,
    up_hbm,
    down_hbm,
    sgate,
    sup,
    sdown,
    out,
    gate,
    up,
    down,
    tokens,
    hidden,
    returned,
    outgoing,
    shidden,
    load_sem,
    own_sem,
    ssend,
    srecv,
    tsend,
    trecv,
    fsend,
    frecv,
    ysend,
    yrecv,
    psend,
    precv,
    gsend,
    grecv,
    rsend,
    rrecv,
):
    e = lax.axis_index("ep")
    q = lax.axis_index("tp")
    z, x = e // 2, e % 2
    y, c = q // 2, q % 2
    sister = (e, y * 2 + (1 - c))
    across = (e, (1 - y) * 2 + c)
    beside = (z * 2 + (1 - x), q)
    rows, width = normed.shape
    half = width // 2
    far = (1 - y) * 2 + c

    def home(s, a):
        return (((z + s) % depth) * 2 + (x if a == 0 else 1 - x), q)

    def copy(src, dst, send, recv, device):
        return pltpu.make_async_remote_copy(
            src_ref=src, dst_ref=dst, send_sem=send, recv_sem=recv, device_id=device, device_id_type=MESH
        )

    loads = [
        pltpu.make_async_copy(src.at[0], dst, load_sem.at[i])
        for i, (src, dst) in enumerate(((gate_hbm, gate), (up_hbm, up), (down_hbm, down)))
    ]
    for load in loads:
        load.start()
    own = [
        pltpu.make_async_copy(normed.at[:, h * half : (h + 1) * half], tokens.at[0, h, 0], own_sem.at[h])
        for h in range(2)
    ]
    for load in own:
        load.start()

    peers = [home(s, a) for s in range(depth) for a in range(2) if (s, a) != (0, 0)]
    peers += [(e, (q + k) % 4) for k in range(1, 4)]
    barrier = pltpu.get_barrier_semaphore()
    for peer in peers:
        pl.semaphore_signal(barrier, inc=1, device_id=peer, device_id_type=MESH)
    pl.semaphore_wait(barrier, len(peers))

    pending = []

    def launch(cp):
        cp.start()
        pending.append(cp)
        return cp

    for load in own:
        load.wait()
    mine = tokens.at[0, c, 0]
    arrive = {}
    arrive[0, 1] = launch(copy(mine, tokens.at[0, c, 1], tsend.at[0, 1], trecv.at[0, 1], beside))
    for s in range(1, depth):
        target = (((z + depth - s) % depth) * 2 + x, q)
        arrive[s, 0] = launch(copy(mine, tokens.at[s, c, 0], tsend.at[s, 0], trecv.at[s, 0], target))

    shared_gate = jnp.dot(normed[...], sgate[...], preferred_element_type=jnp.float32)
    shared_up = jnp.dot(normed[...], sup[...], preferred_element_type=jnp.float32)
    shidden[q] = (silu(shared_gate) * shared_up).astype(jnp.bfloat16)

    swapped = {}

    def pass_on(s, a):
        arrive[s, a].wait_recv()
        block = tokens.at[s, c, a]
        if a == 0:
            arrive[s, 1] = launch(copy(block, tokens.at[s, c, 1], tsend.at[s, 1], trecv.at[s, 1], beside))
        swapped[s, a] = launch(copy(block, tokens.at[s, c, a], fsend.at[s, a], frecv.at[s, a], sister))

    tile = hidden.shape[4]
    ycopies, pcopies = {}, {}

    def first(s):
        for t in range(TILES):
            cols = slice(t * tile, (t + 1) * tile)

            def product(weight):
                total = None
                for h in range(2):
                    block = tokens[s, h].reshape(2 * rows, half)
                    part = jnp.dot(block, weight[h * half : (h + 1) * half, cols], preferred_element_type=jnp.float32)
                    total = part if total is None else total + part
                return total

            hidden[s, q, t] = (silu(product(gate)) * product(up)).astype(jnp.bfloat16)
            block = hidden.at[s, q, t]
            ycopies[s, t] = launch(copy(block, hidden.at[s, q, t], ysend.at[s, t], yrecv.at[s, t], across))
            pcopies[s, t] = launch(copy(block, hidden.at[s, q, t], psend.at[s, t], precv.at[s, t], sister))

    pass_on(0, 1)
    pass_on(1, 0)
    swapped[0, 1].wait_recv()
    loads[0].wait()
    loads[1].wait()
    first(0)
    scopies = []
    for k in range(1, 4):
        scopies.append(
            launch(copy(shidden.at[q], shidden.at[q], ssend.at[k - 1], srecv.at[k - 1], (e, (q + k) % 4)))
        )
    for s in range(1, depth):
        if s + 1 < depth:
            pass_on(s + 1, 0)
        pass_on(s, 1)
        swapped[s, 0].wait_recv()
        swapped[s, 1].wait_recv()
        first(s)

    loads[2].wait()
    homes = {}
    for s in range(depth):
        forwards = []
        for t in range(TILES):
            ycopies[s, t].wait_recv()
            forwards.append(
                launch(copy(hidden.at[s, far, t], hidden.at[s, far, t], gsend.at[s, t], grecv.at[s, t], sister))
            )
            pcopies[s, t].wait_recv()
        for forward in forwards:
            forward.wait_recv()
        total = None
        for k in range(4):
            for t in range(TILES):
                at = (k * TILES + t) * tile
                part = jnp.dot(hidden[s, k, t], down[at : at + tile, :], preferred_element_type=jnp.float32)
                total = part if total is None else total + part
        for a in range(2):
            piece = total[a * rows : (a + 1) * rows].astype(jnp.bfloat16)
            if (s, a) == (0, 0):
                returned[0, 0] = piece
            else:
                outgoing[s, a] = piece
                homes[s, a] = launch(
                    copy(outgoing.at[s, a], returned.at[s, a], rsend.at[s, a], rrecv.at[s, a], home(s, a))
                )

    for cp in scopies:
        cp.wait_recv()
    moe_sum = None
    share = shidden.shape[2]
    for k in range(4):
        part = jnp.dot(shidden[k], sdown[k * share : (k + 1) * share, :], preferred_element_type=jnp.float32)
        moe_sum = part if moe_sum is None else moe_sum + part
    for s in range(depth):
        for a in range(2):
            if (s, a) != (0, 0):
                homes[s, a].wait_recv()
            at = s * 2 + a
            moe_sum = moe_sum + weights[:, at : at + 1] * returned[s, a].astype(jnp.float32)
    out[...] = moe_sum.astype(jnp.bfloat16)
    for cp in pending:
        cp.wait_send()


def moe_fused(normed, routes, route_weights, expert_gate, expert_up, expert_down, shared_gate, shared_up, shared_down):
    rows, width = normed.shape
    depth = lax.axis_size("ep") // 2
    e = lax.axis_index("ep")
    z, x = e // 2, e % 2
    source = jnp.stack([((z + depth - s) % depth) * 2 + (x + a) % 2 for s in range(depth) for a in range(2)])
    weights = jnp.sum(
        jnp.where(routes[:, :, None] == source[None, None, :], route_weights[:, :, None], 0.0), axis=1
    )
    units, columns = expert_gate.shape[2], expert_down.shape[2]
    tile = units // TILES
    bf = jnp.bfloat16
    vmem = pl.BlockSpec(memory_space=pltpu.VMEM)
    hbm = pl.BlockSpec(memory_space=pl.ANY)
    dma = pltpu.SemaphoreType.DMA
    pairs = (depth, 2)
    flops = 2 * depth * 2 * rows * (2 * width * units + 4 * units * columns)
    return pl.pallas_call(
        functools.partial(moe_kernel, depth),
        out_shape=jax.ShapeDtypeStruct((rows, columns), bf),
        in_specs=[vmem, vmem, hbm, hbm, hbm, vmem, vmem, vmem],
        out_specs=vmem,
        scratch_shapes=[
            pltpu.VMEM(expert_gate.shape[1:], bf),
            pltpu.VMEM(expert_up.shape[1:], bf),
            pltpu.VMEM(expert_down.shape[1:], bf),
            pltpu.VMEM((depth, 2, 2, rows, width // 2), bf),
            pltpu.VMEM((depth, 4, TILES, 2 * rows, tile), bf),
            pltpu.VMEM((depth, 2, rows, columns), bf),
            pltpu.VMEM((depth, 2, rows, columns), bf),
            pltpu.VMEM((4, rows, shared_gate.shape[1]), bf),
            dma((3,)),
            dma((2,)),
            dma((3,)),
            dma((3,)),
        ]
        + [dma(pairs)] * 4
        + [dma((depth, TILES))] * 6
        + [dma(pairs)] * 2,
        compiler_params=pltpu.CompilerParams(
            collective_id=0, has_side_effects=True, vmem_limit_bytes=44 * 1024 * 1024
        ),
        cost_estimate=pl.CostEstimate(flops=flops * 2, bytes_accessed=40_000_000, transcendentals=0),
    )(normed, weights, expert_gate, expert_up, expert_down, shared_gate, shared_up, shared_down)


def moe_general(normed, routes, route_weights, expert_gate, expert_up, expert_down, shared_gate, shared_up, shared_down):
    rows_b, per_row = routes.shape
    model_width = normed.shape[1]
    groups = lax.axis_size("ep")
    capacity = 2 * rows_b * per_row // groups
    flat_expert = routes.reshape(-1)
    owner_row = jnp.arange(rows_b * per_row, dtype=jnp.int32) // per_row
    expert_hits = (flat_expert[:, None] == jnp.arange(groups, dtype=jnp.int32)[None, :]).astype(
        jnp.int32
    )
    slot_rank = jnp.sum((jnp.cumsum(expert_hits, axis=0) - expert_hits) * expert_hits, axis=1)
    slot_index = flat_expert * capacity + slot_rank
    outgoing = (
        jnp.zeros((groups * capacity, model_width), jnp.bfloat16)
        .at[slot_index]
        .set(normed[owner_row])
    )
    outgoing = outgoing.reshape(groups, capacity, model_width)
    slot_share = capacity // lax.axis_size("tp")
    own_slots = lax.dynamic_slice_in_dim(outgoing, lax.axis_index("tp") * slot_share, slot_share, 1)
    partial_rows = lax.all_to_all(own_slots, "ep", split_axis=0, concat_axis=0, tiled=True)
    arrived = lax.all_gather(partial_rows, "tp", axis=1, tiled=True)
    arrived_rows = arrived.reshape(groups * capacity, model_width)
    gate_value = jnp.dot(arrived_rows, expert_gate[0], preferred_element_type=jnp.float32)
    upward = jnp.dot(arrived_rows, expert_up[0], preferred_element_type=jnp.float32)
    expert_hidden = (jax.nn.silu(gate_value) * upward).astype(jnp.bfloat16)
    shared_hidden = (
        jax.nn.silu(jnp.dot(normed, shared_gate, preferred_element_type=jnp.float32))
        * jnp.dot(normed, shared_up, preferred_element_type=jnp.float32)
    ).astype(jnp.bfloat16)
    columns = expert_down.shape[2]
    routed_sum = jnp.dot(
        lax.all_gather(expert_hidden, "tp", axis=1, tiled=True),
        expert_down[0],
        preferred_element_type=jnp.float32,
    )
    shared_sum = jnp.dot(
        lax.all_gather(shared_hidden, "tp", axis=1, tiled=True),
        shared_down,
        preferred_element_type=jnp.float32,
    )
    expert_out = routed_sum.astype(jnp.bfloat16).reshape(groups, capacity, columns)
    returned = lax.all_to_all(expert_out, "ep", split_axis=0, concat_axis=0, tiled=True).reshape(
        groups * capacity, columns
    )
    picked = returned[slot_index].astype(jnp.float32) * route_weights.reshape(-1)[:, None]
    moe_sum = jnp.sum(picked.reshape(rows_b, per_row, columns), axis=1) + shared_sum
    return moe_sum.astype(jnp.bfloat16)


def body(
    conv_value,
    conv_gate,
    conv_taps,
    norm_gain,
    norm_shift,
    conv_out_weight,
    moe_input,
    moe_gain,
    routes,
    route_weights,
    expert_gate,
    expert_up,
    expert_down,
    shared_gate,
    shared_up,
    shared_down,
):
    tap_count = conv_taps.shape[0]
    rows_a = conv_value.shape[0]
    glu_rows = (
        conv_value.astype(jnp.float32) * jax.nn.sigmoid(conv_gate.astype(jnp.float32))
    ).astype(jnp.bfloat16)
    before = from_behind(glu_rows[rows_a - (tap_count - 1) :], "ep", 1)
    padded = jnp.concatenate([before, glu_rows], axis=0)
    filtered = jnp.zeros(glu_rows.shape, jnp.float32)
    for offset in range(tap_count):
        filtered = filtered + conv_taps[offset] * padded[offset : offset + rows_a].astype(
            jnp.float32
        )
    row_total, squares = lax.psum(
        (jnp.sum(filtered, axis=1), jnp.sum(filtered * filtered, axis=1)), "tp"
    )
    channels = conv_out_weight.shape[0]
    row_mean = row_total / channels
    row_square = squares / channels
    scaled = (filtered - row_mean[:, None]) * lax.rsqrt(row_square - row_mean * row_mean + 1e-05)[
        :, None
    ]
    conv_hidden = jax.nn.silu(scaled * norm_gain + norm_shift).astype(jnp.bfloat16)
    conv_sum = jnp.dot(
        lax.all_gather(conv_hidden, "tp", axis=1, tiled=True),
        conv_out_weight,
        preferred_element_type=jnp.float32,
    )
    conv_result = conv_sum.astype(jnp.bfloat16)
    inputs = moe_input.astype(jnp.float32)
    normed = (
        inputs * lax.rsqrt(jnp.mean(inputs * inputs, axis=1, keepdims=True) + 1e-06) * moe_gain
    ).astype(jnp.bfloat16)
    dense = lax.axis_size("tp") == 4 and lax.axis_size("ep") in (2, 4, 8)
    moe = moe_fused if dense else moe_general
    moe_result = moe(
        normed, routes, route_weights, expert_gate, expert_up, expert_down, shared_gate, shared_up, shared_down
    )
    return (conv_result, moe_result)


def solution(mesh):
    return jax.shard_map(
        body,
        mesh=mesh,
        in_specs=(
            P("ep", "tp"),
            P("ep", "tp"),
            P(None, "tp"),
            P("tp"),
            P("tp"),
            P(None, "tp"),
            P("ep", None),
            P(),
            P("ep", None),
            P("ep", None),
            P("ep", None, "tp"),
            P("ep", None, "tp"),
            P("ep", None, "tp"),
            P(None, "tp"),
            P(None, "tp"),
            P(None, "tp"),
        ),
        out_specs=(P("ep", "tp"), P("ep", "tp")),
        check_vma=False,
    )
```

time: 222 us -> 140 us (0.63)
  waiting for transfers between devices: 89.1 us -> 0.04 us
  Pallas kernels: 0 us -> 78.9 us
  blocking collectives: 45.5 us -> 6.33 us
  matrix products: 32.5 us -> 3.63 us
  other arithmetic: 11.7 us -> 24.7 us
  local copies, waits for them, and re-layouts: 19.8 us -> 7.07 us
  starting transfers between devices: 9.02 us -> 4.91 us
    pallas_call x0 -> x1, Pallas kernels: none -> 78.9 us  [moe_fused(): pl.pallas_call(functools.partial(moe_kernel, depth), out_shape=jax.ShapeD...]
    all_gather x2 -> x0, waiting for transfers between devices: 74.2 us -> none  [the longest x1 40.6 us: body(): lax.all_gather(expert_hidden, 'tp', axis=1, tiled=True)]
    all_to_all x1 -> x0, blocking collectives: 32.9 us -> none  [body(): lax.all_to_all(own_slots, 'ep', split_axis=0, concat_axis=0, tiled=True)]
    dot_general x6 -> x0, matrix products: 28.9 us -> none  [the longest x1 10 us: body(): jnp.dot(lax.all_gather(expert_hidden, 'tp', axis=1, tiled=True), routed_r...]
    reduce_sum x1, other arithmetic: 4.85 us -> 19.1 us  [body(): jnp.sum(filtered, axis=1)]
    scatter x1 -> x0, local copies, waits for them, and re-layouts: 12.8 us -> none  [body(): outgoing = jnp.zeros((groups * capacity, model_width), jnp.bfloat16).at[s...]
    all_to_all x1 -> x0, waiting for transfers between devices: 12.7 us -> none  [body(): lax.all_to_all(expert_out, 'ep', split_axis=0, concat_axis=0, tiled=True)]
    all_gather x1 -> x0, blocking collectives: 6.1 us -> none  [body(): lax.all_gather(shared_hidden, 'tp', axis=1, tiled=True)]
  transfers between devices with their start and end apart: 5 -> 2, of which waited for: 5 -> 0; matrix products, arithmetic and copies ran while one was open for 10% -> 3% of each run, Pallas kernels for 0% -> 56%
where the time goes in v1:
time: 140 us
  Pallas kernels  78.9 us (56%)
  other arithmetic  24.7 us (18%)
  between operations  14.3 us (10%)
  local copies, waits for them, and re-layouts  7.07 us (5%)
  blocking collectives  6.33 us (5%)
  starting transfers between devices  4.91 us (4%)
  matrix products  3.63 us (3%)
    pallas_call x1, Pallas kernels, moe_fused(): pl.pallas_call(functools.partial(moe_kernel, depth), out_shape=jax.ShapeD...  78.9 us
    reduce_sum x1, other arithmetic, body(): jnp.sum(filtered, axis=1)  19.1 us
    psum x1, blocking collectives, body(): lax.psum((jnp.sum(filtered, axis=1), jnp.sum(filtered * filtered, axis=1)...  6.33 us
    ppermute x1, starting transfers between devices, from_behind(): lax.ppermute(value, axis, [(source, source + steps) for source in range(i...  4.87 us
    unnamed x25, local copies, waits for them, and re-layouts  4.72 us
    dot_general x1, matrix products, body(): jnp.dot(lax.all_gather(conv_hidden, 'tp', axis=1, tiled=True), conv_out_w...  3.63 us
  transfers between devices with their start and end apart: 2, of which 0 were waited for; matrix products, arithmetic and copies ran while one was open for 3% of the time, Pallas kernels for 56%

profile of v1, /device:TPU:0, one launch (start us, length us, event | category | flops | bytes accessed | tf_op | source)
XLA Modules:
  0.0 139.9 jit_solution(583592047588710826)
XLA Ops:
  7.2 0.0 copy-start
  7.2 0.0 copy-start.6
  7.2 0.0 all-gather.2.cloned.1.call-start
  7.3 1.6 %multiply_convert_fusion.1 = bf16[512,512]{1,0:T(8,128)(2,1)S(1)} fusion(bf16[512,512]{1,0:T(8,128)(2,1)} %param.17, bf16[512,512]{1,0:T(8,128)(2,1)} %param.16), kind=kLoop, calls=%fused_computation.38 | loop fusion | flops 1835008 | bytes 1572864 | tf_op jit(solution)/shard_map/convert_element_type | solution.py:331
  8.9 0.0 copy-start.5
  8.9 0.8 copy-done.5
  9.7 4.9 %collective-permute-start = (bf16[30,512]{1,0:T(8,128)(2,1)S(1)}, bf16[30,512]{1,0:T(8,128)(2,1)S(1)}, u32[]{:S(2)}, u32[]{:S(2)}) collective-permute-start(bf16[30,512]{1,0:T(8,128)(2,1)S(1)} %slice.248), channel_id=1, source_target_pairs={{0,4},{4,8},{8,12},{12,16},{16,20},{20,24},{24,28},{1,5},{5,9},{9,... | collective-permute-start | bytes 92168 | tf_op jit(solution)/shard_map/ppermute | solution.py:17
  14.6 1.0 fusion.34
  15.6 1.1 fusion.33
  16.8 0.0 copy-done.6
  16.8 0.2 fusion
  17.0 0.0 copy-start.11
  17.0 0.0 copy-start.7
  17.1 0.1 stack.35
  17.2 0.0 collective-permute-done
  17.2 0.0 copy-start.2
  17.2 0.0 copy-start.3
  17.2 19.1 %fusion.32 = (f32[512]{0:T(512)S(1)}, f32[512]{0:T(512)S(1)}, f32[512,512]{1,0:T(8,128)}) fusion(bf16[512,512]{1,0:T(8,128)(2,1)} %copy-done.5, f32[512]{0:T(512)S(1)} %bitcast.51, bf16[30,512]{1,0:T(8,128)(2,1)S(1)} %collective-permute-done, f32[512]{0:T(512)S(1)} %bitcast.52, f32[512]{0:T(512)S(1)} %bitcast.54, f32[512]{0:T(512)S(1)} %bitcast.55, ...), kind=kLoop, calls=%fused_computation.78 | loop fusion | flops 48495616 | bytes 1671168 | tf_op jit(solution)/shard_map/reduce_sum | solution.py:340
  36.3 6.3 %all-reduce = (f32[512]{0:T(512)S(1)}, f32[512]{0:T(512)S(1)}) all-reduce(f32[512]{0:T(512)S(1)} %get-tuple-element.3, f32[512]{0:T(512)S(1)} %get-tuple-element.2), channel_id=1, replica_groups=mesh['ep'=8,'tp'=4] {'tp'}, use_global_device_ids=true, to_apply=%region_3.0 | all-reduce | flops 1024 | bytes 8192 | tf_op jit(solution)/shard_map/psum | solution.py:339
  42.7 2.4 %multiply_convert_fusion = bf16[512,512]{1,0:T(8,128)(2,1)} fusion(f32[512,512]{1,0:T(8,128)} %get-tuple-element.6, f32[512]{0:T(512)S(1)} %copy-done.8, f32[512]{0:T(512)S(1)} %copy-done.9, f32[512]{0:T(512)S(1)} %get-tuple-element.39, f32[512]{0:T(512)S(1)} %get-tuple-element.38), kind=kLoop, calls=%fused_computation.35 | loop fusion | flops 2359296 | bytes 1581056 | tf_op jit(solution)/shard_map/convert_element_type | solution.py:348
  45.1 0.0 all-gather.2.cloned.1.call-update
  45.1 0.0 copy-done.10
  45.1 0.1 select_reduce_fusion
  45.2 0.1 copy.20.weights
  45.3 1.2 fusion.2.normed
  46.6 0.0 copy-start.1
  46.6 2.2 %copy-done.1 = bf16[1,2048,1024]{2,1,0:T(8,128)(2,1)S(1)} copy-done((bf16[1,2048,1024]{2,1,0:T(8,128)(2,1)S(1)}, bf16[1,2048,1024]{2,1,0:T(8,128)(2,1)}, u32[]{:S(2)}) %copy-start.1) | copy-done | bytes 4194328
  48.8 1.0 copy-done.4
  49.8 78.9 %shard_map.167 = bf16[128,512]{1,0:T(8,128)(2,1)S(1)} custom-call(bf16[128,2048]{1,0:T(8,128)(2,1)S(1)} %fusion.2.normed, f32[128,8]{1,0:T(8,128)S(1)} %copy.20.weights, bf16[1,2048,1024]{2,1,0:T(8,128)(2,1)S(1)} %copy-done.1, bf16[1,2048,1024]{2,1,0:T(8,128)(2,1)} %up_hbm.1, bf16[1,4096,512]{2,1,0:T(8,128)(2,1)} %down_hbm.1, ...), custom_call_target="tpu_custom_call" | custom-call | flops 25769803776 | bytes 40000000 | tf_op jit(solution)/shard_map/pallas_call | solution.py:230
  128.8 0.0 all-gather.2.cloned.1.call-done
  128.8 3.6 %convolution_convert_fusion = bf16[512,512]{1,0:T(8,128)(2,1)} fusion(bf16[512,2048]{1,0:T(8,128)(2,1)} %all-gather.2.cloned.1.call-done, bf16[2048,512]{1,0:T(8,128)(2,1)S(1)} %copy-done), kind=kOutput, calls=%fused_computation.31 | convolution fusion | flops 1074003968 | bytes 4718592 | tf_op jit(solution)/shard_map/dot_general | solution.py:349
  132.4 0.7 copy.22
  (14 shorter events, 0.0 us)
Async XLA Ops:
  7.2 121.6 %copy-start = (bf16[2048,512]{1,0:T(8,128)(2,1)S(1)}, bf16[2048,512]{1,0:T(8,128)(2,1)}, u32[]{:S(2)}) copy-start(bf16[2048,512]{1,0:T(8,128)(2,1)} %param.21) | copy-start | bytes 6291460
  7.2 9.6 %copy-start.6 = (bf16[128,2048]{1,0:T(8,128)(2,1)S(1)}, bf16[128,2048]{1,0:T(8,128)(2,1)}, u32[]{:S(2)}) copy-start(bf16[128,2048]{1,0:T(8,128)(2,1)} %param.22) | copy-start | bytes 1572868
  7.2 35.5 %copy-start.8 = (f32[512]{0:T(512)S(1)}, f32[512]{0:T(512)}, u32[]{:S(2)}) copy-start(f32[512]{0:T(512)} %param.20) | copy-start | bytes 6148
  7.2 35.4 %copy-start.9 = (f32[512]{0:T(512)S(1)}, f32[512]{0:T(512)}, u32[]{:S(2)}) copy-start(f32[512]{0:T(512)} %param.19) | copy-start | bytes 6148
  7.2 121.6 %all-gather.2.cloned.1.call-start = ((), (), s32[]{:S(2)}) async-start(), calls=%async_computation | async-start | bytes 2621440 | tf_op jit(solution)/shard_map/all_gather | solution.py:350
  8.9 0.8 copy-start.5
  9.7 7.5 %collective-permute-start = (bf16[30,512]{1,0:T(8,128)(2,1)S(1)}, bf16[30,512]{1,0:T(8,128)(2,1)S(1)}, u32[]{:S(2)}, u32[]{:S(2)}) collective-permute-start(bf16[30,512]{1,0:T(8,128)(2,1)S(1)} %slice.248), channel_id=1, source_target_pairs={{0,4},{4,8},{8,12},{12,16},{16,20},{20,24},{24,28},{1,5},{5,9},{9,... | collective-permute-start | bytes 92168 | tf_op jit(solution)/shard_map/ppermute | solution.py:17
  17.0 28.2 %copy-start.10 = (f32[128,4]{0,1:T(4,128)S(1)}, f32[128,4]{0,1:T(4,128)}, u32[]{:S(2)}) copy-start(f32[128,4]{0,1:T(4,128)} %param.25) | copy-start | bytes 6148
  17.0 28.2 %copy-start.11 = (s32[128,4]{0,1:T(4,128)S(1)}, s32[128,4]{0,1:T(4,128)}, u32[]{:S(2)}) copy-start(s32[128,4]{0,1:T(4,128)} %param.24) | copy-start | bytes 6148
  17.0 28.3 %copy-start.7 = (f32[2048]{0:T(1024)S(1)}, f32[2048]{0:T(1024)}, u32[]{:S(2)}) copy-start(f32[2048]{0:T(1024)} %param.23) | copy-start | bytes 24580
  17.2 29.4 %copy-start.2 = (bf16[2048,128]{1,0:T(8,128)(2,1)S(1)}, bf16[2048,128]{1,0:T(8,128)(2,1)}, u32[]{:S(2)}) copy-start(bf16[2048,128]{1,0:T(8,128)(2,1)} %sgate.1) | copy-start | bytes 1572868
  17.2 29.4 %copy-start.3 = (bf16[2048,128]{1,0:T(8,128)(2,1)S(1)}, bf16[2048,128]{1,0:T(8,128)(2,1)}, u32[]{:S(2)}) copy-start(bf16[2048,128]{1,0:T(8,128)(2,1)} %sup.1) | copy-start | bytes 1572868
  46.6 2.2 %copy-start.1 = (bf16[1,2048,1024]{2,1,0:T(8,128)(2,1)S(1)}, bf16[1,2048,1024]{2,1,0:T(8,128)(2,1)}, u32[]{:S(2)}) copy-start(bf16[1,2048,1024]{2,1,0:T(8,128)(2,1)} %gate_hbm.1) | copy-start | bytes 12582916
  48.8 1.0 copy-start.4
Sparse Core Ops, SparseCore 0:
  45.2 24.1 all-gather.1

commit v2 on v1

--- a/solution.py
+++ b/solution.py
@@ -9,6 +9,7 @@
 
 MESH = pl.DeviceIdType.MESH
 TILES = 2
+CHUNK = 64
 
 
 def from_behind(value, axis, steps):
@@ -28,10 +29,30 @@
     gate_hbm,
     up_hbm,
     down_hbm,
+    sgate_hbm,
+    sup_hbm,
+    sdown_hbm,
+    value_hbm,
+    cgate_hbm,
+    cweight_hbm,
+    taps,
+    gain,
+    shift,
+    conv_out,
+    out,
     sgate,
     sup,
     sdown,
-    out,
+    value,
+    cgate,
+    cweight,
+    padded,
+    filtered,
+    stats,
+    tail,
+    halo,
+    rowsums,
+    chidden,
     gate,
     up,
     down,
@@ -56,6 +77,10 @@
     grecv,
     rsend,
     rrecv,
+    msend,
+    mrecv,
+    csend,
+    crecv,
 ):
     e = lax.axis_index("ep")
     q = lax.axis_index("tp")
@@ -77,8 +102,20 @@
         )
 
     loads = [
-        pltpu.make_async_copy(src.at[0], dst, load_sem.at[i])
-        for i, (src, dst) in enumerate(((gate_hbm, gate), (up_hbm, up), (down_hbm, down)))
+        pltpu.make_async_copy(src, dst, load_sem.at[i])
+        for i, (src, dst) in enumerate(
+            (
+                (value_hbm, value),
+                (cgate_hbm, cgate),
+                (sgate_hbm, sgate),
+                (sup_hbm, sup),
+                (gate_hbm.at[0], gate),
+                (up_hbm.at[0], up),
+                (cweight_hbm, cweight),
+                (down_hbm.at[0], down),
+                (sdown_hbm, sdown),
+            )
+        )
     ]
     for load in loads:
         load.start()
@@ -112,9 +149,71 @@
         target = (((z + depth - s) % depth) * 2 + x, q)
         arrive[s, 0] = launch(copy(mine, tokens.at[s, c, 0], tsend.at[s, 0], trecv.at[s, 0], target))
 
+    rows_a, channels = value.shape
+    tap_count, edge = taps.shape[0], halo.shape[0]
+    lead = edge - (tap_count - 1)
+    chunks = rows_a // CHUNK
+
+    def chunk_of(i):
+        return pl.multiple_of(i * CHUNK, CHUNK)
+
+    def glu(i, carry):
+        at = pl.ds(chunk_of(i), CHUNK)
+        gated = value[at, :].astype(jnp.float32) * (1.0 / (1.0 + jnp.exp(-cgate[at, :].astype(jnp.float32))))
+        rounded = gated.astype(jnp.bfloat16).astype(jnp.float32)
+        padded[pl.ds(pl.multiple_of(i * CHUNK + edge, 8), CHUNK), :] = rounded
+        return carry
+
+    loads[0].wait()
+    loads[1].wait()
+    lax.fori_loop(0, chunks, glu, 0)
+    tail[...] = padded[rows_a:, :].astype(jnp.bfloat16)
+    count = 2 * depth
+    edge_copy = launch(copy(tail, halo, csend.at[0], crecv.at[0], ((e + 1) % count, q)))
+
+    loads[2].wait()
+    loads[3].wait()
     shared_gate = jnp.dot(normed[...], sgate[...], preferred_element_type=jnp.float32)
     shared_up = jnp.dot(normed[...], sup[...], preferred_element_type=jnp.float32)
     shidden[q] = (silu(shared_gate) * shared_up).astype(jnp.bfloat16)
+
+    edge_copy.wait_recv()
+    padded[0:edge, :] = jnp.where(e == 0, 0.0, halo[...].astype(jnp.float32))
+    lane = lax.broadcasted_iota(jnp.int32, (CHUNK, 128), 1)
+
+    def convolve(i, carry):
+        start = chunk_of(i)
+        at = pl.ds(start, CHUNK)
+        sums, squares = jnp.zeros((CHUNK, 128), jnp.float32), jnp.zeros((CHUNK, 128), jnp.float32)
+        for column in range(0, channels, 128):
+            cols = slice(column, column + 128)
+            window = padded[pl.ds(start, CHUNK + edge), cols]
+            total = jnp.zeros((CHUNK, 128), jnp.float32)
+            for b in range(8):
+                size = CHUNK + (8 if b else 0)
+                part = None
+                for a in range(edge // 8 + 1):
+                    j = 8 * a + b - lead
+                    if 0 <= j < tap_count:
+                        term = taps[j : j + 1, cols] * window[8 * a : 8 * a + size]
+                        part = term if part is None else part + term
+                if b:
+                    part = pltpu.roll(part, size - b, 0)[:CHUNK]
+                total = total + part
+            filtered[at, cols] = total
+            sums = sums + total
+            squares = squares + total * total
+        row_sum = jnp.sum(sums, axis=1, keepdims=True)
+        row_squares = jnp.sum(squares, axis=1, keepdims=True)
+        stats[at, :] = jnp.where(lane == 0, row_sum, jnp.where(lane == 1, row_squares, 0.0))
+        return carry
+
+    lax.fori_loop(0, chunks, convolve, 0)
+    rowsums[q] = stats[...].T[:8]
+    mcopies = [
+        launch(copy(rowsums.at[q], rowsums.at[q], msend.at[k - 1], mrecv.at[k - 1], (e, (q + k) % 4)))
+        for k in range(1, 4)
+    ]
 
     swapped = {}
 
@@ -148,9 +247,27 @@
     pass_on(0, 1)
     pass_on(1, 0)
     swapped[0, 1].wait_recv()
-    loads[0].wait()
-    loads[1].wait()
+    loads[4].wait()
+    loads[5].wait()
     first(0)
+
+    for cp in mcopies:
+        cp.wait_recv()
+    whole = rowsums[0] + rowsums[1] + rowsums[2] + rowsums[3]
+    stats[...] = jnp.concatenate([whole, jnp.zeros((120, rows_a), jnp.float32)], axis=0).T
+    total_channels = channels * 4
+
+    def normalise(i, carry):
+        at = pl.ds(chunk_of(i), CHUNK)
+        both = stats[at, :] / total_channels
+        mean, square = both[:, 0:1], both[:, 1:2]
+        scaled = (filtered[at, :] - mean) * lax.rsqrt(square - mean * mean + 1e-05)
+        chidden[q, at, :] = silu(scaled * gain[...] + shift[...]).astype(jnp.bfloat16)
+        return carry
+
+    lax.fori_loop(0, chunks, normalise, 0)
+    cacross = launch(copy(chidden.at[q], chidden.at[q], csend.at[1], crecv.at[1], across))
+    csister = launch(copy(chidden.at[q], chidden.at[q], csend.at[2], crecv.at[2], sister))
     scopies = []
     for k in range(1, 4):
         scopies.append(
@@ -164,7 +281,27 @@
         swapped[s, 1].wait_recv()
         first(s)
 
-    loads[2].wait()
+    cacross.wait_recv()
+    cpassed = launch(copy(chidden.at[far], chidden.at[far], csend.at[3], crecv.at[3], sister))
+    csister.wait_recv()
+    loads[6].wait()
+    cpassed.wait_recv()
+
+    def project(i, carry):
+        at = pl.ds(pl.multiple_of(i * 256, 256), 256)
+        product = None
+        for k in range(4):
+            part = jnp.dot(
+                chidden[k, at, :],
+                cweight[k * channels : (k + 1) * channels, :],
+                preferred_element_type=jnp.float32,
+            )
+            product = part if product is None else product + part
+        conv_out[at, :] = product.astype(jnp.bfloat16)
+        return carry
+
+    lax.fori_loop(0, rows_a // 256, project, 0)
+    loads[7].wait()
     homes = {}
     for s in range(depth):
         forwards = []
@@ -194,6 +331,7 @@
 
     for cp in scopies:
         cp.wait_recv()
+    loads[8].wait()
     moe_sum = None
     share = shidden.shape[2]
     for k in range(4):
@@ -210,7 +348,12 @@
         cp.wait_send()
 
 
-def moe_fused(normed, routes, route_weights, expert_gate, expert_up, expert_down, shared_gate, shared_up, shared_down):
+def fused(
+    conv, normed, routes, route_weights, expert_gate, expert_up, expert_down, shared_gate, shared_up, shared_down
+):
+    value, cgate, taps, gain, shift, cweight = conv
+    rows_a, channels = value.shape
+    edge = -(-(taps.shape[0] - 1) // 8) * 8
     rows, width = normed.shape
     depth = lax.axis_size("ep") // 2
     e = lax.axis_index("ep")
@@ -229,10 +372,26 @@
     flops = 2 * depth * 2 * rows * (2 * width * units + 4 * units * columns)
     return pl.pallas_call(
         functools.partial(moe_kernel, depth),
-        out_shape=jax.ShapeDtypeStruct((rows, columns), bf),
-        in_specs=[vmem, vmem, hbm, hbm, hbm, vmem, vmem, vmem],
-        out_specs=vmem,
+        out_shape=(
+            jax.ShapeDtypeStruct((rows_a, cweight.shape[1]), bf),
+            jax.ShapeDtypeStruct((rows, columns), bf),
+        ),
+        in_specs=[vmem] * 2 + [hbm] * 9 + [vmem] * 3,
+        out_specs=(vmem, vmem),
         scratch_shapes=[
+            pltpu.VMEM(shared_gate.shape, bf),
+            pltpu.VMEM(shared_up.shape, bf),
+            pltpu.VMEM(shared_down.shape, bf),
+            pltpu.VMEM(value.shape, bf),
+            pltpu.VMEM(cgate.shape, bf),
+            pltpu.VMEM(cweight.shape, bf),
+            pltpu.VMEM((rows_a + edge, channels), jnp.float32),
+            pltpu.VMEM((rows_a, channels), jnp.float32),
+            pltpu.VMEM((rows_a, 128), jnp.float32),
+            pltpu.VMEM((edge, channels), bf),
+            pltpu.VMEM((edge, channels), bf),
+            pltpu.VMEM((4, 8, rows_a), jnp.float32),
+            pltpu.VMEM((4, rows_a, channels), bf),
             pltpu.VMEM(expert_gate.shape[1:], bf),
             pltpu.VMEM(expert_up.shape[1:], bf),
             pltpu.VMEM(expert_down.shape[1:], bf),
@@ -241,19 +400,36 @@
             pltpu.VMEM((depth, 2, rows, columns), bf),
             pltpu.VMEM((depth, 2, rows, columns), bf),
             pltpu.VMEM((4, rows, shared_gate.shape[1]), bf),
-            dma((3,)),
+            dma((9,)),
             dma((2,)),
             dma((3,)),
             dma((3,)),
         ]
         + [dma(pairs)] * 4
         + [dma((depth, TILES))] * 6
-        + [dma(pairs)] * 2,
+        + [dma(pairs)] * 2
+        + [dma((3,))] * 2
+        + [dma((4,))] * 2,
         compiler_params=pltpu.CompilerParams(
-            collective_id=0, has_side_effects=True, vmem_limit_bytes=44 * 1024 * 1024
+            collective_id=0, has_side_effects=True, vmem_limit_bytes=56 * 1024 * 1024
         ),
         cost_estimate=pl.CostEstimate(flops=flops * 2, bytes_accessed=40_000_000, transcendentals=0),
-    )(normed, weights, expert_gate, expert_up, expert_down, shared_gate, shared_up, shared_down)
+    )(
+        normed,
+        weights,
+        expert_gate,
+        expert_up,
+        expert_down,
+        shared_gate,
+        shared_up,
+        shared_down,
+        value,
+        cgate,
+        cweight,
+        taps,
+        gain.reshape(1, -1),
+        shift.reshape(1, -1),
+    )
 
 
 def moe_general(normed, routes, route_weights, expert_gate, expert_up, expert_down, shared_gate, shared_up, shared_down):
@@ -306,6 +482,37 @@
     return moe_sum.astype(jnp.bfloat16)
 
 
+def conv_general(conv_value, conv_gate, conv_taps, norm_gain, norm_shift, conv_out_weight):
+    tap_count = conv_taps.shape[0]
+    rows_a = conv_value.shape[0]
+    glu_rows = (
+        conv_value.astype(jnp.float32) * jax.nn.sigmoid(conv_gate.astype(jnp.float32))
+    ).astype(jnp.bfloat16)
+    before = from_behind(glu_rows[rows_a - (tap_count - 1) :], "ep", 1)
+    padded = jnp.concatenate([before, glu_rows], axis=0)
+    filtered = jnp.zeros(glu_rows.shape, jnp.float32)
+    for offset in range(tap_count):
+        filtered = filtered + conv_taps[offset] * padded[offset : offset + rows_a].astype(
+            jnp.float32
+        )
+    row_total, squares = lax.psum(
+        (jnp.sum(filtered, axis=1), jnp.sum(filtered * filtered, axis=1)), "tp"
+    )
+    channels = conv_out_weight.shape[0]
+    row_mean = row_total / channels
+    row_square = squares / channels
+    scaled = (filtered - row_mean[:, None]) * lax.rsqrt(row_square - row_mean * row_mean + 1e-05)[
+        :, None
+    ]
+    conv_hidden = jax.nn.silu(scaled * norm_gain + norm_shift).astype(jnp.bfloat16)
+    conv_sum = jnp.dot(
+        lax.all_gather(conv_hidden, "tp", axis=1, tiled=True),
+        conv_out_weight,
+        preferred_element_type=jnp.float32,
+    )
+    return conv_sum.astype(jnp.bfloat16)
+
+
 def body(
     conv_value,
     conv_gate,
@@ -324,44 +531,15 @@
     shared_up,
     shared_down,
 ):
-    tap_count = conv_taps.shape[0]
-    rows_a = conv_value.shape[0]
-    glu_rows = (
-        conv_value.astype(jnp.float32) * jax.nn.sigmoid(conv_gate.astype(jnp.float32))
-    ).astype(jnp.bfloat16)
-    before = from_behind(glu_rows[rows_a - (tap_count - 1) :], "ep", 1)
-    padded = jnp.concatenate([before, glu_rows], axis=0)
-    filtered = jnp.zeros(glu_rows.shape, jnp.float32)
-    for offset in range(tap_count):
-        filtered = filtered + conv_taps[offset] * padded[offset : offset + rows_a].astype(
-            jnp.float32
-        )
-    row_total, squares = lax.psum(
-        (jnp.sum(filtered, axis=1), jnp.sum(filtered * filtered, axis=1)), "tp"
-    )
-    channels = conv_out_weight.shape[0]
-    row_mean = row_total / channels
-    row_square = squares / channels
-    scaled = (filtered - row_mean[:, None]) * lax.rsqrt(row_square - row_mean * row_mean + 1e-05)[
-        :, None
-    ]
-    conv_hidden = jax.nn.silu(scaled * norm_gain + norm_shift).astype(jnp.bfloat16)
-    conv_sum = jnp.dot(
-        lax.all_gather(conv_hidden, "tp", axis=1, tiled=True),
-        conv_out_weight,
-        preferred_element_type=jnp.float32,
-    )
-    conv_result = conv_sum.astype(jnp.bfloat16)
     inputs = moe_input.astype(jnp.float32)
     normed = (
         inputs * lax.rsqrt(jnp.mean(inputs * inputs, axis=1, keepdims=True) + 1e-06) * moe_gain
     ).astype(jnp.bfloat16)
-    dense = lax.axis_size("tp") == 4 and lax.axis_size("ep") in (2, 4, 8)
-    moe = moe_fused if dense else moe_general
-    moe_result = moe(
-        normed, routes, route_weights, expert_gate, expert_up, expert_down, shared_gate, shared_up, shared_down
-    )
-    return (conv_result, moe_result)
+    conv = (conv_value, conv_gate, conv_taps, norm_gain, norm_shift, conv_out_weight)
+    moe = (routes, route_weights, expert_gate, expert_up, expert_down, shared_gate, shared_up, shared_down)
+    if lax.axis_size("tp") == 4 and lax.axis_size("ep") in (2, 4, 8):
+        return fused(conv, normed, *moe)
+    return (conv_general(*conv), moe_general(normed, *moe))
 
 
 def solution(mesh):

time: 140 us -> 116 us (0.83)
  the two profiles are of different devices: /device:TPU:0 before, /device:TPU:10 now
where the time goes in v2:
time: 116 us
  Pallas kernels  107 us (92%)
  local copies, waits for them, and re-layouts  4.25 us (4%)
  other arithmetic  4.04 us (3%)
    pallas_call x1, Pallas kernels, fused(): pl.pallas_call(functools.partial(moe_kernel, depth), out_shape=(jax.Shape...  107 us
    unnamed x2, local copies, waits for them, and re-layouts  3.44 us

profile of v2, /device:TPU:10, one launch (start us, length us, event | category | flops | bytes accessed | tf_op | source)
XLA Modules:
  0.0 115.7 jit_solution(9722587431067962753)
XLA Ops:
  0.7 0.1 stack.35
  0.8 1.2 %fusion = f32[128]{0:T(128)S(1)} fusion(bf16[128,2048]{1,0:T(8,128)(2,1)} %param.22), kind=kLoop, calls=%fused_computation.2 | loop fusion | flops 786304 | bytes 524800 | tf_op jit(solution)/shard_map/reduce_sum | solution.py:536
  2.1 0.8 select_reduce_fusion
  2.8 0.7 copy.20.weights
  3.6 2.0 %fusion.2.normed = bf16[128,2048]{1,0:T(8,128)(2,1)} fusion(bf16[128,2048]{1,0:T(8,128)(2,1)} %param.22, f32[2048]{0:T(1024)} %param.23, f32[128]{0:T(128)S(1)} %add_rsqrt_fusion), kind=kLoop, calls=%fused_computation.4 | loop fusion | flops 1048576 | bytes 1057280 | tf_op jit(solution)/shard_map/convert_element_type | solution.py:537
  5.6 106.6 %shard_map.167 = (bf16[512,512]{1,0:T(8,128)(2,1)}, bf16[128,512]{1,0:T(8,128)(2,1)}) custom-call(bf16[128,2048]{1,0:T(8,128)(2,1)} %fusion.2.normed, f32[128,8]{1,0:T(8,128)} %copy.20.weights, bf16[1,2048,1024]{2,1,0:T(8,128)(2,1)} %gate_hbm.1, bf16[1,2048,1024]{2,1,0:T(8,128)(2,1)} %up_hbm.1, bf16[1,4096,512]{2,1,0:T(8,128)(2,1)} %down_hbm.1, ...), custom_call_target="tpu_custom_call" | custom-call | flops 25769803776 | bytes 40000000 | tf_op jit(solution)/shard_map/pallas_call | solution.py:373
  112.2 1.9 %copy.23 = bf16[512,512]{1,0:T(8,128)(2,1)} copy(bf16[512,512]{1,0:T(8,128)(2,1)} %get-tuple-element.4) | data formatting | bytes 1048576
  114.1 1.6 %copy.24 = bf16[128,512]{1,0:T(8,128)(2,1)} copy(bf16[128,512]{1,0:T(8,128)(2,1)} %get-tuple-element.5) | data formatting | bytes 262144
  (1 shorter events, 0.0 us)

commit v3 on v2

--- a/solution.py
+++ b/solution.py
@@ -177,6 +177,42 @@
     shared_up = jnp.dot(normed[...], sup[...], preferred_element_type=jnp.float32)
     shidden[q] = (silu(shared_gate) * shared_up).astype(jnp.bfloat16)
 
+    swapped = {}
+
+    def pass_on(s, a):
+        arrive[s, a].wait_recv()
+        block = tokens.at[s, c, a]
+        if a == 0:
+            arrive[s, 1] = launch(copy(block, tokens.at[s, c, 1], tsend.at[s, 1], trecv.at[s, 1], beside))
+        swapped[s, a] = launch(copy(block, tokens.at[s, c, a], fsend.at[s, a], frecv.at[s, a], sister))
+
+    tile = hidden.shape[4]
+    ycopies, pcopies = {}, {}
+
+    def first(s):
+        for t in range(TILES):
+            cols = slice(t * tile, (t + 1) * tile)
+
+            def product(weight):
+                total = None
+                for h in range(2):
+                    block = tokens[s, h].reshape(2 * rows, half)
+                    part = jnp.dot(block, weight[h * half : (h + 1) * half, cols], preferred_element_type=jnp.float32)
+                    total = part if total is None else total + part
+                return total
+
+            hidden[s, q, t] = (silu(product(gate)) * product(up)).astype(jnp.bfloat16)
+            block = hidden.at[s, q, t]
+            ycopies[s, t] = launch(copy(block, hidden.at[s, q, t], ysend.at[s, t], yrecv.at[s, t], across))
+            pcopies[s, t] = launch(copy(block, hidden.at[s, q, t], psend.at[s, t], precv.at[s, t], sister))
+
+    pass_on(0, 1)
+    pass_on(1, 0)
+    swapped[0, 1].wait_recv()
+    loads[4].wait()
+    loads[5].wait()
+    first(0)
+
     edge_copy.wait_recv()
     padded[0:edge, :] = jnp.where(e == 0, 0.0, halo[...].astype(jnp.float32))
     lane = lax.broadcasted_iota(jnp.int32, (CHUNK, 128), 1)
@@ -215,59 +251,6 @@
         for k in range(1, 4)
     ]
 
-    swapped = {}
-
-    def pass_on(s, a):
-        arrive[s, a].wait_recv()
-        block = tokens.at[s, c, a]
-        if a == 0:
-            arrive[s, 1] = launch(copy(block, tokens.at[s, c, 1], tsend.at[s, 1], trecv.at[s, 1], beside))
-        swapped[s, a] = launch(copy(block, tokens.at[s, c, a], fsend.at[s, a], frecv.at[s, a], sister))
-
-    tile = hidden.shape[4]
-    ycopies, pcopies = {}, {}
-
-    def first(s):
-        for t in range(TILES):
-            cols = slice(t * tile, (t + 1) * tile)
-
-            def product(weight):
-                total = None
-                for h in range(2):
-                    block = tokens[s, h].reshape(2 * rows, half)
-                    part = jnp.dot(block, weight[h * half : (h + 1) * half, cols], preferred_element_type=jnp.float32)
-                    total = part if total is None else total + part
-                return total
-
-            hidden[s, q, t] = (silu(product(gate)) * product(up)).astype(jnp.bfloat16)
-            block = hidden.at[s, q, t]
-            ycopies[s, t] = launch(copy(block, hidden.at[s, q, t], ysend.at[s, t], yrecv.at[s, t], across))
-            pcopies[s, t] = launch(copy(block, hidden.at[s, q, t], psend.at[s, t], precv.at[s, t], sister))
-
-    pass_on(0, 1)
-    pass_on(1, 0)
-    swapped[0, 1].wait_recv()
-    loads[4].wait()
-    loads[5].wait()
-    first(0)
-
-    for cp in mcopies:
-        cp.wait_recv()
-    whole = rowsums[0] + rowsums[1] + rowsums[2] + rowsums[3]
-    stats[...] = jnp.concatenate([whole, jnp.zeros((120, rows_a), jnp.float32)], axis=0).T
-    total_channels = channels * 4
-
-    def normalise(i, carry):
-        at = pl.ds(chunk_of(i), CHUNK)
-        both = stats[at, :] / total_channels
-        mean, square = both[:, 0:1], both[:, 1:2]
-        scaled = (filtered[at, :] - mean) * lax.rsqrt(square - mean * mean + 1e-05)
-        chidden[q, at, :] = silu(scaled * gain[...] + shift[...]).astype(jnp.bfloat16)
-        return carry
-
-    lax.fori_loop(0, chunks, normalise, 0)
-    cacross = launch(copy(chidden.at[q], chidden.at[q], csend.at[1], crecv.at[1], across))
-    csister = launch(copy(chidden.at[q], chidden.at[q], csend.at[2], crecv.at[2], sister))
     scopies = []
     for k in range(1, 4):
         scopies.append(
@@ -280,6 +263,24 @@
         swapped[s, 0].wait_recv()
         swapped[s, 1].wait_recv()
         first(s)
+        if s == 1:
+            for cp in mcopies:
+                cp.wait_recv()
+            whole = rowsums[0] + rowsums[1] + rowsums[2] + rowsums[3]
+            stats[...] = jnp.concatenate([whole, jnp.zeros((120, rows_a), jnp.float32)], axis=0).T
+            total_channels = channels * 4
+
+            def normalise(i, carry):
+                at = pl.ds(chunk_of(i), CHUNK)
+                both = stats[at, :] / total_channels
+                mean, square = both[:, 0:1], both[:, 1:2]
+                scaled = (filtered[at, :] - mean) * lax.rsqrt(square - mean * mean + 1e-05)
+                chidden[q, at, :] = silu(scaled * gain[...] + shift[...]).astype(jnp.bfloat16)
+                return carry
+
+            lax.fori_loop(0, chunks, normalise, 0)
+            cacross = launch(copy(chidden.at[q], chidden.at[q], csend.at[1], crecv.at[1], across))
+            csister = launch(copy(chidden.at[q], chidden.at[q], csend.at[2], crecv.at[2], sister))
 
     cacross.wait_recv()
     cpassed = launch(copy(chidden.at[far], chidden.at[far], csend.at[3], crecv.at[3], sister))

time: 116 us -> 103 us (0.89)
  the two profiles are of different devices: /device:TPU:10 before, /device:TPU:0 now
where the time goes in v3:
time: 103 us
  Pallas kernels  93.7 us (91%)
  local copies, waits for them, and re-layouts  4.25 us (4%)
  other arithmetic  4.04 us (4%)
    pallas_call x1, Pallas kernels, fused(): pl.pallas_call(functools.partial(moe_kernel, depth), out_shape=(jax.Shape...  93.7 us
    unnamed x2, local copies, waits for them, and re-layouts  3.44 us

profile of v3, /device:TPU:0, one launch (start us, length us, event | category | flops | bytes accessed | tf_op | source)
XLA Modules:
  0.0 102.7 jit_solution(15464607529236591176)
XLA Ops:
  0.7 0.1 stack.35
  0.8 1.2 %fusion = f32[128]{0:T(128)S(1)} fusion(bf16[128,2048]{1,0:T(8,128)(2,1)} %param.22), kind=kLoop, calls=%fused_computation.2 | loop fusion | flops 786304 | bytes 524800 | tf_op jit(solution)/shard_map/reduce_sum | solution.py:537
  2.1 0.8 select_reduce_fusion
  2.8 0.7 copy.20.weights
  3.6 2.0 %fusion.2.normed = bf16[128,2048]{1,0:T(8,128)(2,1)} fusion(bf16[128,2048]{1,0:T(8,128)(2,1)} %param.22, f32[2048]{0:T(1024)} %param.23, f32[128]{0:T(128)S(1)} %add_rsqrt_fusion), kind=kLoop, calls=%fused_computation.4 | loop fusion | flops 1048576 | bytes 1057280 | tf_op jit(solution)/shard_map/convert_element_type | solution.py:538
  5.6 93.7 %shard_map.167 = (bf16[512,512]{1,0:T(8,128)(2,1)}, bf16[128,512]{1,0:T(8,128)(2,1)}) custom-call(bf16[128,2048]{1,0:T(8,128)(2,1)} %fusion.2.normed, f32[128,8]{1,0:T(8,128)} %copy.20.weights, bf16[1,2048,1024]{2,1,0:T(8,128)(2,1)} %gate_hbm.1, bf16[1,2048,1024]{2,1,0:T(8,128)(2,1)} %up_hbm.1, bf16[1,4096,512]{2,1,0:T(8,128)(2,1)} %down_hbm.1, ...), custom_call_target="tpu_custom_call" | custom-call | flops 25769803776 | bytes 40000000 | tf_op jit(solution)/shard_map/pallas_call | solution.py:374
  99.3 1.9 %copy.23 = bf16[512,512]{1,0:T(8,128)(2,1)} copy(bf16[512,512]{1,0:T(8,128)(2,1)} %get-tuple-element.4) | data formatting | bytes 1048576
  101.2 1.6 %copy.24 = bf16[128,512]{1,0:T(8,128)(2,1)} copy(bf16[128,512]{1,0:T(8,128)(2,1)} %get-tuple-element.5) | data formatting | bytes 262144
  (1 shorter events, 0.0 us)
